TPU v7x, 32 devices: a whole 2x2x4 slice. The times are simulated.
32 devices in a mesh: fs: 16 (over z, y, core), tp: 2 (over x).
Axes of the slice: x: 2, y: 2, z: 4, core: 2. Of those that a mesh axis runs over, the one named last changes fastest.
Arguments:
- prompt: bfloat16 [2048, 2048], P('fs'), may hold values from -6 to 6
- norm_gain: float32 [2048], P('fs'), may hold values from 0.1 to 1.9
- gate_train: float32 [2048, 32768], P('fs', 'tp'), may hold values from -0.125 to 0.125
- up_train: float32 [2048, 32768], P('fs', 'tp'), may hold values from -0.125 to 0.125
- down_train: float32 [2048, 32768], P('fs', 'tp'), may hold values from -0.25 to 0.25
- common_gate_train: float32 [2048, 512], P('fs', 'tp'), may hold values from -0.125 to 0.125
- common_up_train: float32 [2048, 512], P('fs', 'tp'), may hold values from -0.125 to 0.125
- common_down_train: float32 [2048, 512], P('fs', 'tp'), may hold values from -0.25 to 0.25
- route_ids: int32 [2048, 6], P('fs'), may hold values from 0 to 63, all different within a row; in each aligned block of 128 rows (0 to 127, 128 to 255, ...) at most 16 rows name the same one
- route_weights: float32 [2048, 6], P('fs'), may hold values from 0.1 to 1
Outputs:
- mixture: bfloat16 [2048, 2048], P('fs', 'tp')
- gate_serve: bfloat16 [64, 512, 2048], P('fs', 'tp')
- up_serve: bfloat16 [64, 512, 2048], P('fs', 'tp')
- down_serve: bfloat16 [64, 512, 2048], P('fs', 'tp')
- common_gate_serve: bfloat16 [512, 2048], P('tp')
- common_up_serve: bfloat16 [512, 2048], P('tp')
- common_down_serve: bfloat16 [512, 2048], P('tp')
Inputs may be any that keep to these rules, and one draw needn't show every extreme that they name: `route_ids`: each row names 6 different experts. Among the rows of one index of fs no expert is named more than 16 times, and in every draw some expert is named exactly 16 times by the rows of some index.
All inputs are finite; a program needn't handle non-finite values.
Results may differ from a plain program's by a relative error of at most 0.011.
Values may be sent and summed in bfloat16 or wider, within the bound.
A program may use at most 128 MiB of HBM per device.

v0:
```python
import jax
import jax.numpy as jnp
from jax import lax
from jax.sharding import PartitionSpec as P

FF = 512
E = 64
TOP_K = 6
CAP = 16
epsilon = 1e-06


def shortened(x):
    return jax.tree.map(lambda a: a.astype(jnp.bfloat16) if a.dtype == jnp.float32 else a, x)


def local(
    prompt,
    norm_gain,
    gate_train,
    up_train,
    down_train,
    common_gate_train,
    common_up_train,
    common_down_train,
    route_ids,
    route_weights,
):
    tp_count = lax.axis_size("tp")
    fs_count = lax.axis_size("fs")
    width_rows = gate_train.shape[0]
    local_experts_tp = gate_train.shape[1] // FF
    unit_block = FF // tp_count
    gain_col = norm_gain[:, None]

    def arrange(low):
        sectioned = low.reshape(width_rows, local_experts_tp, tp_count, unit_block)
        sectioned = jnp.transpose(sectioned, (2, 1, 3, 0))
        return sectioned.reshape(tp_count, local_experts_tp, unit_block * width_rows)

    crossed = (
        lax.all_to_all(
            arrange((gate_train * gain_col).astype(jnp.bfloat16)),
            "tp",
            split_axis=0,
            concat_axis=1,
            tiled=True,
        ),
        lax.all_to_all(
            arrange((up_train * gain_col).astype(jnp.bfloat16)),
            "tp",
            split_axis=0,
            concat_axis=1,
            tiled=True,
        ),
        lax.all_to_all(
            arrange(down_train.astype(jnp.bfloat16)), "tp", split_axis=0, concat_axis=1, tiled=True
        ),
    )
    all_experts = crossed[0].shape[1]
    spread = lax.all_to_all(
        shortened(
            tuple((item.reshape(all_experts, 1, unit_block * width_rows) for item in crossed))
        ),
        "fs",
        split_axis=0,
        concat_axis=1,
        tiled=True,
    )

    def finish(arrived_weights):
        owned = arrived_weights.shape[0]
        sectioned = arrived_weights.reshape(owned, fs_count, unit_block, width_rows)
        return jnp.transpose(sectioned, (0, 2, 1, 3)).reshape(
            owned, unit_block, fs_count * width_rows
        )

    gate_serve, up_serve, down_serve = (finish(item) for item in spread)
    common_block = common_gate_train.shape[1]
    common_low = jnp.stack(
        [
            jnp.transpose(common_gate_train * gain_col),
            jnp.transpose(common_up_train * gain_col),
            jnp.transpose(common_down_train),
        ]
    ).astype(jnp.bfloat16)
    common_all = lax.all_gather(
        common_low.reshape(1, 3 * common_block * width_rows), "fs", axis=0, tiled=True
    )
    common_all = jnp.transpose(
        common_all.reshape(fs_count, 3, common_block, width_rows), (1, 2, 0, 3)
    )
    common_all = common_all.reshape(3, common_block, fs_count * width_rows)
    common_gate_serve, common_up_serve, common_down_serve = (
        common_all[0],
        common_all[1],
        common_all[2],
    )
    values = prompt.astype(jnp.float32)
    normed = (
        values * lax.rsqrt(jnp.mean(values * values, axis=1, keepdims=True) + epsilon)
    ).astype(jnp.bfloat16)
    flat_ids = route_ids.reshape(-1)
    onehot = (flat_ids[:, None] == jnp.arange(E, dtype=jnp.int32)[None, :]).astype(jnp.int32)
    before = jnp.cumsum(onehot, axis=0) - onehot
    slot_of = jnp.sum(before * onehot, axis=1)
    target = flat_ids * CAP + slot_of
    model_width = normed.shape[1]
    buffer = (
        jnp.zeros((E * CAP, model_width), jnp.bfloat16)
        .at[target]
        .set(jnp.repeat(normed, TOP_K, axis=0))
    )
    buffer = buffer.reshape(E, CAP, model_width)
    common_gate = jnp.einsum(
        "td,fd->tf", normed, common_gate_serve, preferred_element_type=jnp.float32
    )
    common_up = jnp.einsum("td,fd->tf", normed, common_up_serve, preferred_element_type=jnp.float32)
    common_hidden = (jax.nn.silu(common_gate) * common_up).astype(jnp.bfloat16)
    common_partial = jnp.dot(
        common_hidden, common_down_serve, preferred_element_type=jnp.float32
    ).astype(jnp.bfloat16)
    whole_gate, whole_up, whole_down = (
        lax.all_gather(gate_serve, "tp", axis=1, tiled=True),
        lax.all_gather(up_serve, "tp", axis=1, tiled=True),
        lax.all_gather(down_serve, "tp", axis=1, tiled=True),
    )
    share = CAP // tp_count
    first_slot = lax.axis_index("tp") * share
    my_slots = lax.dynamic_slice_in_dim(buffer, first_slot, share, 1)
    arrived = lax.all_to_all(my_slots, "fs", split_axis=0, concat_axis=1, tiled=True)
    gate_value = jnp.einsum("erd,efd->erf", arrived, whole_gate, preferred_element_type=jnp.float32)
    up_value = jnp.einsum("erd,efd->erf", arrived, whole_up, preferred_element_type=jnp.float32)
    hidden = (jax.nn.silu(gate_value) * up_value).astype(jnp.bfloat16)
    owned, slot_rows = (hidden.shape[0], hidden.shape[1])
    blocked_hidden = hidden.reshape(owned, slot_rows, tp_count, unit_block)
    blocked_down = whole_down.reshape(owned, tp_count, unit_block, model_width)
    partial_value = jnp.einsum(
        "ermf,emfd->merd", blocked_hidden, blocked_down, preferred_element_type=jnp.float32
    ).astype(jnp.bfloat16)
    expert_out = jnp.sum(partial_value.astype(jnp.float32), axis=0).astype(jnp.bfloat16)
    returned = lax.all_to_all(expert_out, "fs", split_axis=1, concat_axis=0, tiled=True)
    inside = (slot_of >= first_slot) & (slot_of < first_slot + share)
    local_index = jnp.where(inside, flat_ids * share + slot_of - first_slot, 0)
    picked = returned.reshape(E * share, model_width)[local_index].astype(jnp.float32)
    pair_weights = jnp.where(inside, route_weights.reshape(-1), 0.0)
    weighted_part = jnp.sum(
        (picked * pair_weights[:, None]).reshape(-1, TOP_K, model_width), axis=1
    )
    weighted, common_sum = (
        lax.psum_scatter(weighted_part, "tp", scatter_dimension=1, tiled=True),
        lax.psum_scatter(common_partial.astype(jnp.float32), "tp", scatter_dimension=1, tiled=True),
    )
    common_out = common_sum.astype(jnp.bfloat16)
    mixture = (weighted + common_out.astype(jnp.float32)).astype(jnp.bfloat16)
    return (
        mixture,
        gate_serve,
        up_serve,
        down_serve,
        common_gate_serve,
        common_up_serve,
        common_down_serve,
    )


def solution(mesh):
    in_specs = (
        P("fs", None),
        P("fs"),
        P("fs", "tp"),
        P("fs", "tp"),
        P("fs", "tp"),
        P("fs", "tp"),
        P("fs", "tp"),
        P("fs", "tp"),
        P("fs", None),
        P("fs", None),
    )
    out_specs = (
        P("fs", "tp"),
        P("fs", "tp", None),
        P("fs", "tp", None),
        P("fs", "tp", None),
        P("tp", None),
        P("tp", None),
        P("tp", None),
    )
    return jax.shard_map(local, mesh=mesh, in_specs=in_specs, out_specs=out_specs, check_vma=False)
```

profile of v0, /device:TPU:0, one launch (start us, length us, event | category | flops | bytes accessed | tf_op | source)
XLA Modules:
  0.0 861.1 jit_solution(5667237024494821347)
XLA Ops:
  7.2 10.8 %multiply_convert_fusion.1 = (bf16[128,16384]{1,0:T(8,128)(2,1)}, bf16[128,16384]{1,0:T(8,128)(2,1)}) fusion(f32[128,16384]{1,0:T(8,128)} %param.12, f32[128]{0:T(128)} %param.11, f32[128,16384]{1,0:T(8,128)} %param.13), kind=kLoop, calls=%fused_computation.6 | loop fusion | flops 8388608 | bytes 25166336 | tf_op jit(solution)/shard_map/convert_element_type | solution.py:43
  25.7 11.3 %copy.100 = bf16[128,32,2,256]{0,3,1,2:T(8,128)(2,1)} copy(bf16[128,32,2,256]{3,2,1,0:T(2,128)(2,1)} %reshape.235) | data formatting | bytes 8388608 | tf_op jit(solution)/shard_map/reshape | solution.py:37
  63.7 11.3 %copy.108 = bf16[128,32,2,256]{0,3,1,2:T(8,128)(2,1)} copy(bf16[128,32,2,256]{3,2,1,0:T(2,128)(2,1)} %reshape.246) | data formatting | bytes 8388608 | tf_op jit(solution)/shard_map/reshape | solution.py:37
  82.2 16.6 %all-to-all-done.1 = bf16[2,32,32768]{2,1,0:T(8,128)(2,1)} async-done(((bf16[2,32,32768]{2,1,0:T(8,128)(2,1)}), bf16[2,32,32768]{2,1,0:T(8,128)(2,1)}, u32[]{:S(2)}, u32[]{:S(2)}) %all-to-all-start.1) | async-done | bytes 4194336 | tf_op jit(solution)/shard_map/all_to_all | solution.py:42
  104.4 7.8 reshape.240
  112.2 11.3 %copy.104 = bf16[128,32,2,256]{0,3,1,2:T(8,128)(2,1)} copy(bf16[128,32,2,256]{3,2,1,0:T(2,128)(2,1)} %reshape.240) | data formatting | bytes 8388608 | tf_op jit(solution)/shard_map/reshape | solution.py:37
  130.8 20.7 %all-to-all-done.5 = bf16[2,32,32768]{2,1,0:T(8,128)(2,1)} async-done(((bf16[2,32,32768]{2,1,0:T(8,128)(2,1)}), bf16[2,32,32768]{2,1,0:T(8,128)(2,1)}, u32[]{:S(2)}, u32[]{:S(2)}) %all-to-all-start.5) | async-done | bytes 4194336 | tf_op jit(solution)/shard_map/all_to_all | solution.py:56
  164.5 7.8 reshape.287
  172.3 31.1 %all-to-all-done.3 = bf16[2,32,32768]{2,1,0:T(8,128)(2,1)} async-done(((bf16[2,32,32768]{2,1,0:T(8,128)(2,1)}), bf16[2,32,32768]{2,1,0:T(8,128)(2,1)}, u32[]{:S(2)}, u32[]{:S(2)}) %all-to-all-start.3) | async-done | bytes 4194336 | tf_op jit(solution)/shard_map/all_to_all | solution.py:49
  215.9 7.9 reshape.291
  223.8 62.9 %all-to-all-done.6 = bf16[16,2,65536]{2,1,0:T(2,128)(2,1)} async-done(((bf16[16,2,65536]{2,1,0:T(2,128)(2,1)}), bf16[16,2,65536]{2,1,0:T(2,128)(2,1)}, u32[]{:S(2)}, u32[]{:S(2)}) %all-to-all-start.6) | async-done | bytes 4194336 | tf_op jit(solution)/shard_map/all_to_all | solution.py:61
  286.7 19.7 %all-to-all-start.2 = ((bf16[16,2,65536]{2,1,0:T(2,128)(2,1)}), bf16[16,2,65536]{2,1,0:T(2,128)(2,1)}, u32[]{:S(2)}, u32[]{:S(2)}) async-start(bf16[16,2,65536]{2,1,0:T(2,128)(2,1)} %reshape.291), calls=%async_computation.2 | async-start | bytes 8388608 | tf_op jit(solution)/shard_map/all_to_all | solution.py:61
  306.6 12.3 %reshape.288 = bf16[64,1,32768]{2,1,0:T(2,128)(2,1)} reshape(bf16[16,2,65536]{2,1,0:T(2,128)(2,1)} %all-to-all-done.6) | data formatting | bytes 8388608
  318.9 26.1 %reduce.5 = bf16[64,32768]{1,0:T(8,128)(2,1)} reduce(bf16[64,1,32768]{2,1,0:T(2,128)(2,1)} %reshape.288, bf16[]{:T(256)} %constant.38), dimensions={1}, to_apply=%all_to_all.91.reduce_sub_computation | reduce | bytes 8388610 | tf_op jit(solution)/shard_map/all_to_all | solution.py:61
  352.2 8.4 reshape.277
  373.6 8.3 reshape.289
  383.9 19.7 %all-to-all-start.4 = ((bf16[16,2,65536]{2,1,0:T(2,128)(2,1)}), bf16[16,2,65536]{2,1,0:T(2,128)(2,1)}, u32[]{:S(2)}, u32[]{:S(2)}) async-start(bf16[16,2,65536]{2,1,0:T(2,128)(2,1)} %reshape.289), calls=%async_computation.4 | async-start | bytes 8388608 | tf_op jit(solution)/shard_map/all_to_all | solution.py:61
  403.7 12.4 %reshape.292 = bf16[64,1,32768]{2,1,0:T(2,128)(2,1)} reshape(bf16[16,2,65536]{2,1,0:T(2,128)(2,1)} %all-to-all-done.2) | data formatting | bytes 8388608
  416.1 26.1 %reduce.3 = bf16[64,32768]{1,0:T(8,128)(2,1)} reduce(bf16[64,1,32768]{2,1,0:T(2,128)(2,1)} %reshape.292, bf16[]{:T(256)} %constant.38), dimensions={1}, to_apply=%all_to_all.83.reduce_sub_computation | reduce | bytes 8388610 | tf_op jit(solution)/shard_map/all_to_all | solution.py:61
  449.3 8.4 reshape.275
  462.9 18.3 %all-to-all-done.4 = bf16[16,2,65536]{2,1,0:T(2,128)(2,1)} async-done(((bf16[16,2,65536]{2,1,0:T(2,128)(2,1)}), bf16[16,2,65536]{2,1,0:T(2,128)(2,1)}, u32[]{:S(2)}, u32[]{:S(2)}) %all-to-all-start.4) | async-done | bytes 4194336 | tf_op jit(solution)/shard_map/all_to_all | solution.py:61
  481.2 12.7 %reshape.290 = bf16[64,1,32768]{2,1,0:T(2,128)(2,1)} reshape(bf16[16,2,65536]{2,1,0:T(2,128)(2,1)} %all-to-all-done.4) | data formatting | bytes 8388608
  493.9 26.1 %reduce.4 = bf16[64,32768]{1,0:T(8,128)(2,1)} reduce(bf16[64,1,32768]{2,1,0:T(2,128)(2,1)} %reshape.290, bf16[]{:T(256)} %constant.38), dimensions={1}, to_apply=%all_to_all.87.reduce_sub_computation | reduce | bytes 8388610 | tf_op jit(solution)/shard_map/all_to_all | solution.py:61
  527.1 8.4 reshape.276
  553.0 9.4 %scatter_custom_fusion = bf16[1024,2048]{1,0:T(8,128)(2,1)} fusion(s32[768]{0:T(1024)S(1)} %get-tuple-element.29, bf16[768,2048]{1,0:T(8,128)(2,1)S(1)} %reshape.267, bf16[]{:T(256)} %constant.11.clone.1), kind=kCustom, calls=%fused_computation.17 | custom fusion | bytes 4194306 | tf_op jit(solution)/shard_map/scatter | solution.py:112
  565.6 19.3 %all-to-all-start = ((bf16[64,8,2048]{2,1,0:T(8,128)(2,1)}), bf16[64,8,2048]{2,1,0:T(8,128)(2,1)S(1)}, u32[]{:S(2)}, u32[]{:S(2)}) async-start(bf16[64,8,2048]{2,1,0:T(8,128)(2,1)} %constant_dynamic-slice_fusion), calls=%async_computation | async-start | bytes 4194304 | tf_op jit(solution)/shard_map/all_to_all | solution.py:131
  586.6 12.0 %copy.112 = bf16[4,512,2048]{2,1,0:T(8,128)(2,1)} copy(bf16[4,512,2048]{1,2,0:T(8,128)(2,1)} %all-gather.10.cloned.1.call-done) | data formatting | bytes 16777216 | tf_op jit(solution)/shard_map/all_gather | solution.py:126
  598.6 27.3 %all-to-all-done = bf16[64,8,2048]{2,1,0:T(8,128)(2,1)S(1)} async-done(((bf16[64,8,2048]{2,1,0:T(8,128)(2,1)}), bf16[64,8,2048]{2,1,0:T(8,128)(2,1)S(1)}, u32[]{:S(2)}, u32[]{:S(2)}) %all-to-all-start) | async-done | bytes 2097184 | tf_op jit(solution)/shard_map/all_to_all | solution.py:131
  632.2 51.4 %all-gather.8.cloned.1.call-done = bf16[4,512,2048]{2,1,0:T(8,128)(2,1)} async-done(((bf16[4,256,2048]{2,1,0:T(8,128)(2,1)}), bf16[4,512,2048]{2,1,0:T(8,128)(2,1)}) %all-gather.8.cloned.1.call-update) | async-done | bytes 8388624 | tf_op jit(solution)/shard_map/all_gather | solution.py:125
  700.3 79.5 %all-gather.12.cloned.1.call-done = bf16[16,1,98304]{2,1,0:T(2,128)(2,1)} async-done(((bf16[1,1,98304]{2,1,0:T(2,128)(2,1)}), bf16[16,1,98304]{2,1,0:T(2,128)(2,1)}) %all-gather.12.cloned.1.call-update) | async-done | bytes 3145744 | tf_op jit(solution)/shard_map/all_gather | solution.py:87
  779.8 18.5 %reduce.7 = bf16[16,98304]{1,0:T(8,128)(2,1)S(1)} reduce(bf16[16,1,98304]{2,1,0:T(2,128)(2,1)} %all-gather.12.cloned.1.call-done, bf16[]{:T(256)} %constant.38), dimensions={1}, to_apply=%all-gather.reduce_sub_computation | reduce | bytes 6291458 | tf_op jit(solution)/shard_map/all_gather | solution.py:87
  840.0 12.1 %reduce-scatter.3.cloned.1.call-done = f32[128,1024]{1,0:T(8,128)} async-done(((f32[128,2048]{1,0:T(8,128)}), f32[128,1024]{1,0:T(8,128)}) %reduce-scatter.3.cloned.1.call-update) | async-done | bytes 524304 | tf_op jit(solution)/shard_map/reduce_scatter | solution.py:151
  (114 shorter events, 210.6 us)
Async XLA Ops:
  44.4 54.5 %all-to-all-start.1 = ((bf16[2,32,32768]{2,1,0:T(8,128)(2,1)}), bf16[2,32,32768]{2,1,0:T(8,128)(2,1)}, u32[]{:S(2)}, u32[]{:S(2)}) async-start(bf16[2,32,32768]{2,1,0:T(8,128)(2,1)} %reshape.236), calls=%async_computation.1 | async-start | bytes 8388608 | tf_op jit(solution)/shard_map/all_to_all | solution.py:42
  98.8 52.7 %all-to-all-start.5 = ((bf16[2,32,32768]{2,1,0:T(8,128)(2,1)}), bf16[2,32,32768]{2,1,0:T(8,128)(2,1)}, u32[]{:S(2)}, u32[]{:S(2)}) async-start(bf16[2,32,32768]{2,1,0:T(8,128)(2,1)} %reshape.247), calls=%async_computation.5 | async-start | bytes 8388608 | tf_op jit(solution)/shard_map/all_to_all | solution.py:56
  151.5 51.9 %all-to-all-start.3 = ((bf16[2,32,32768]{2,1,0:T(8,128)(2,1)}), bf16[2,32,32768]{2,1,0:T(8,128)(2,1)}, u32[]{:S(2)}, u32[]{:S(2)}) async-start(bf16[2,32,32768]{2,1,0:T(8,128)(2,1)} %reshape.241), calls=%async_computation.3 | async-start | bytes 8388608 | tf_op jit(solution)/shard_map/all_to_all | solution.py:49
  203.4 83.3 %all-to-all-start.6 = ((bf16[16,2,65536]{2,1,0:T(2,128)(2,1)}), bf16[16,2,65536]{2,1,0:T(2,128)(2,1)}, u32[]{:S(2)}, u32[]{:S(2)}) async-start(bf16[16,2,65536]{2,1,0:T(2,128)(2,1)} %reshape.287), calls=%async_computation.6 | async-start | bytes 8388608 | tf_op jit(solution)/shard_map/all_to_all | solution.py:61
  286.7 97.2 %all-to-all-start.2 = ((bf16[16,2,65536]{2,1,0:T(2,128)(2,1)}), bf16[16,2,65536]{2,1,0:T(2,128)(2,1)}, u32[]{:S(2)}, u32[]{:S(2)}) async-start(bf16[16,2,65536]{2,1,0:T(2,128)(2,1)} %reshape.291), calls=%async_computation.2 | async-start | bytes 8388608 | tf_op jit(solution)/shard_map/all_to_all | solution.py:61
  306.4 280.2 %all-gather.10.cloned.1.call-start = ((), (), s32[]{:S(2)}) async-start(), calls=%async_computation.12 | async-start | bytes 12582912 | tf_op jit(solution)/shard_map/all_gather | solution.py:126
  383.9 97.2 %all-to-all-start.4 = ((bf16[16,2,65536]{2,1,0:T(2,128)(2,1)}), bf16[16,2,65536]{2,1,0:T(2,128)(2,1)}, u32[]{:S(2)}, u32[]{:S(2)}) async-start(bf16[16,2,65536]{2,1,0:T(2,128)(2,1)} %reshape.289), calls=%async_computation.4 | async-start | bytes 8388608 | tf_op jit(solution)/shard_map/all_to_all | solution.py:61
  403.6 222.3 %all-gather.6.cloned.1.call-start = ((), (), s32[]{:S(2)}) async-start(), calls=%async_computation.10 | async-start | bytes 12582912 | tf_op jit(solution)/shard_map/all_gather | solution.py:124
  462.6 221.0 %all-gather.8.cloned.1.call-start = ((), (), s32[]{:S(2)}) async-start(), calls=%async_computation.11 | async-start | bytes 12582912 | tf_op jit(solution)/shard_map/all_gather | solution.py:125
  540.4 0.7 copy-start.10
  540.4 3.7 copy-start.6
  544.5 0.8 copy-start.5
  562.4 22.9 %copy-start.7 = (f32[128,256]{1,0:T(8,128)S(1)}, f32[128,256]{1,0:T(8,128)}, u32[]{:S(2)}) copy-start(f32[128,256]{1,0:T(8,128)} %param.15) | copy-start | bytes 393220
  562.4 22.9 %copy-start.8 = (f32[128,256]{1,0:T(8,128)S(1)}, f32[128,256]{1,0:T(8,128)}, u32[]{:S(2)}) copy-start(f32[128,256]{1,0:T(8,128)} %param.16) | copy-start | bytes 393220
  562.4 22.9 %copy-start.9 = (f32[128,256]{1,0:T(8,128)S(1)}, f32[128,256]{1,0:T(8,128)}, u32[]{:S(2)}) copy-start(f32[128,256]{1,0:T(8,128)} %param.17) | copy-start | bytes 393220
  562.4 23.0 %copy-start.12 = (f32[128]{0:T(128)S(1)}, f32[128]{0:T(128)}, u32[]{:S(2)}) copy-start(f32[128]{0:T(128)} %param.11) | copy-start | bytes 1540
  565.6 60.3 %all-to-all-start = ((bf16[64,8,2048]{2,1,0:T(8,128)(2,1)}), bf16[64,8,2048]{2,1,0:T(8,128)(2,1)S(1)}, u32[]{:S(2)}, u32[]{:S(2)}) async-start(bf16[64,8,2048]{2,1,0:T(8,128)(2,1)} %constant_dynamic-slice_fusion), calls=%async_computation | async-start | bytes 4194304 | tf_op jit(solution)/shard_map/all_to_all | solution.py:131
  584.9 194.8 %all-gather.12.cloned.1.call-start = ((), (), s32[]{:S(2)}) async-start(), calls=%async_computation.15 | async-start | bytes 6684672 | tf_op jit(solution)/shard_map/all_gather | solution.py:87
  683.6 6.5 copy-start.4
  694.4 113.8 %all-to-all-start.7 = ((bf16[4,128,2048]{2,0,1:T(4,128)(2,1)}), bf16[4,128,2048]{2,0,1:T(4,128)(2,1)}, u32[]{:S(2)}, u32[]{:S(2)}) async-start(bf16[4,128,2048]{2,0,1:T(4,128)(2,1)} %copy.115), calls=%async_computation.7 | async-start | bytes 4194304 | tf_op jit(solution)/shard_map/all_to_all | solution.py:142
  700.1 140.0 %reduce-scatter.5.cloned.1.call-start = ((), (), s32[]{:S(2)}) async-start(), calls=%async_computation.14 | async-start | bytes 1572864 | tf_op jit(solution)/shard_map/reduce_scatter | solution.py:152
  801.1 6.7 copy-start
  801.1 6.9 copy-start.11
  803.0 7.9 copy-start.2
  807.8 44.3 %reduce-scatter.3.cloned.1.call-start = ((), (), s32[]{:S(2)}) async-start(), calls=%async_computation.13 | async-start | bytes 1572864 | tf_op jit(solution)/shard_map/reduce_scatter | solution.py:151
  821.9 9.1 %copy-start.1 = (bf16[1,256,16,128]{1,3,2,0:T(8,128)(2,1)S(1)}, bf16[1,256,16,128]{1,3,2,0:T(8,128)(2,1)}, u32[]{:S(2)}) copy-start(bf16[1,256,16,128]{1,3,2,0:T(8,128)(2,1)} %copy-done) | copy-start | bytes 3145732
  829.5 2.9 copy-start.3
Sparse Core Ops, SparseCore 0:
  367.0 104.2 all-gather.9
  473.4 103.9 all-gather.5
  579.5 103.9 all-gather.7
  686.3 93.4 all-gather.11
  807.9 21.5 reduce-scatter.4
  831.6 20.3 reduce-scatter.2
where the time goes:
time: 875 us; the launch traced here: 861 us
  waiting for transfers between devices  322 us (37%)
  local copies, waits for them, and re-layouts  271 us (31%)
  other arithmetic  146 us (17%)
  starting transfers between devices  88.1 us (10%)
  matrix products  18.9 us (2%)
  between operations  14.7 us (2%)
    all_to_all x3, waiting for transfers between devices, local(): lax.all_to_all(shortened(tuple((item.reshape(all_experts, 1, unit_block *...  83.2 us
    all_gather x1, waiting for transfers between devices, local(): lax.all_gather(common_low.reshape(1, 3 * common_block * width_rows), 'fs'...  79.5 us
    all_to_all x3, other arithmetic, local(): lax.all_to_all(shortened(tuple((item.reshape(all_experts, 1, unit_block *...  78.3 us
    unnamed x40, local copies, waits for them, and re-layouts  75 us
    reshape x6, local copies, waits for them, and re-layouts, arrange(): sectioned = low.reshape(width_rows, local_experts_tp, tp_count, unit_block)  57.2 us
    all_gather x1, waiting for transfers between devices, local(): lax.all_gather(up_serve, 'tp', axis=1, tiled=True)  51.4 us
    all_to_all x3, starting transfers between devices, local(): lax.all_to_all(shortened(tuple((item.reshape(all_experts, 1, unit_block *...  45.1 us
    all_to_all x1, waiting for transfers between devices, local(): lax.all_to_all(arrange((up_train * gain_col).astype(jnp.bfloat16)), 'tp',...  31.1 us
  transfers between devices with their start and end apart: 14, of which 10 were waited for; matrix products, arithmetic and copies ran while one was open for 43% of the time, Pallas kernels for 0%

commit v1 on v0

--- a/solution.py
+++ b/solution.py
@@ -122,7 +122,7 @@
     ).astype(jnp.bfloat16)
     whole_gate, whole_up, whole_down = (
         lax.all_gather(gate_serve, "tp", axis=1, tiled=True),
-        lax.all_gather(up_serve, "tp", axis=1, tiled=True),
+        jnp.concatenate(lax.all_gather(up_serve, "tp"), axis=1),
         lax.all_gather(down_serve, "tp", axis=1, tiled=True),
     )
     share = CAP // tp_count

time: 875 us -> 901 us (1.030)
  local copies, waits for them, and re-layouts: 271 us -> 293 us
    all_gather x1, waiting for transfers between devices: 51.4 us -> 0.02 us  [local(): lax.all_gather(up_serve, 'tp')]
    all_gather x1, waiting for transfers between devices: 0.01 us -> 50 us  [local(): lax.all_gather(gate_serve, 'tp', axis=1, tiled=True)]
    all_to_all x3, waiting for transfers between devices: 83.2 us -> 131 us  [local(): lax.all_to_all(shortened(tuple((item.reshape(all_experts, 1, unit_block *...]
    all_to_all x1, waiting for transfers between devices: 16.6 us -> 0.01 us  [local(): lax.all_to_all(arrange((gate_train * gain_col).astype(jnp.bfloat16)), 'tp...]
    all_to_all x1, waiting for transfers between devices: 31.1 us -> 16.6 us  [local(): lax.all_to_all(arrange((up_train * gain_col).astype(jnp.bfloat16)), 'tp',...]
    all_to_all x1, waiting for transfers between devices: 20.7 us -> 31.9 us  [local(): lax.all_to_all(arrange(down_train.astype(jnp.bfloat16)), 'tp', split_axis...]
    unnamed x40 -> x45, local copies, waits for them, and re-layouts: 75 us -> 80.4 us
  transfers between devices with their start and end apart: 14 -> 14, of which waited for: 10 -> 9; matrix products, arithmetic and copies ran while one was open for 43% -> 44% of each run, Pallas kernels for 0% -> 0%
where the time goes in v1:
time: 901 us; the launch traced here: 889 us
  waiting for transfers between devices  331 us (37%)
  local copies, waits for them, and re-layouts  293 us (33%)
  other arithmetic  146 us (16%)
  starting transfers between devices  89 us (10%)
  matrix products  15.7 us (2%)
  between operations  14.7 us (2%)
    all_to_all x3, waiting for transfers between devices, local(): lax.all_to_all(shortened(tuple((item.reshape(all_experts, 1, unit_block *...  131 us
    unnamed x45, local copies, waits for them, and re-layouts  80.4 us
    all_to_all x3, other arithmetic, local(): lax.all_to_all(shortened(tuple((item.reshape(all_experts, 1, unit_block *...  78.3 us
    all_gather x1, waiting for transfers between devices, local(): lax.all_gather(common_low.reshape(1, 3 * common_block * width_rows), 'fs'...  76.2 us
    reshape x6, local copies, waits for them, and re-layouts, arrange(): sectioned = low.reshape(width_rows, local_experts_tp, tp_count, unit_block)  57.2 us
    all_gather x1, waiting for transfers between devices, local(): lax.all_gather(gate_serve, 'tp', axis=1, tiled=True)  50 us
    all_to_all x3, starting transfers between devices, local(): lax.all_to_all(shortened(tuple((item.reshape(all_experts, 1, unit_block *...  45.8 us
    all_to_all x1, waiting for transfers between devices, local(): lax.all_to_all(arrange(down_train.astype(jnp.bfloat16)), 'tp', split_axis...  31.9 us
  transfers between devices with their start and end apart: 14, of which 9 were waited for; matrix products, arithmetic and copies ran while one was open for 44% of the time, Pallas kernels for 0%

profile of v1, /device:TPU:0, one launch (start us, length us, event | category | flops | bytes accessed | tf_op | source)
XLA Modules:
  0.0 888.9 jit_solution(17843416166543938858)
XLA Ops:
  7.2 10.8 %multiply_convert_fusion.1 = (bf16[128,16384]{1,0:T(8,128)(2,1)}, bf16[128,16384]{1,0:T(8,128)(2,1)}) fusion(f32[128,16384]{1,0:T(8,128)} %param.12, f32[128]{0:T(128)} %param.11, f32[128,16384]{1,0:T(8,128)} %param.13), kind=kLoop, calls=%fused_computation.6 | loop fusion | flops 8388608 | bytes 25166336 | tf_op jit(solution)/shard_map/convert_element_type | solution.py:43
  25.7 11.3 %copy.110 = bf16[128,32,2,256]{0,3,1,2:T(8,128)(2,1)} copy(bf16[128,32,2,256]{3,2,1,0:T(2,128)(2,1)} %reshape.246) | data formatting | bytes 8388608 | tf_op jit(solution)/shard_map/reshape | solution.py:37
  63.7 11.3 %copy.116 = bf16[128,32,2,256]{0,3,1,2:T(8,128)(2,1)} copy(bf16[128,32,2,256]{3,2,1,0:T(2,128)(2,1)} %reshape.253) | data formatting | bytes 8388608 | tf_op jit(solution)/shard_map/reshape | solution.py:37
  82.2 16.6 %all-to-all-done.3 = bf16[2,32,32768]{2,1,0:T(8,128)(2,1)} async-done(((bf16[2,32,32768]{2,1,0:T(8,128)(2,1)}), bf16[2,32,32768]{2,1,0:T(8,128)(2,1)}, u32[]{:S(2)}, u32[]{:S(2)}) %all-to-all-start.3) | async-done | bytes 4194336 | tf_op jit(solution)/shard_map/all_to_all | solution.py:49
  111.8 7.9 reshape.297
  119.6 31.9 %all-to-all-done.5 = bf16[2,32,32768]{2,1,0:T(8,128)(2,1)} async-done(((bf16[2,32,32768]{2,1,0:T(8,128)(2,1)}), bf16[2,32,32768]{2,1,0:T(8,128)(2,1)}, u32[]{:S(2)}, u32[]{:S(2)}) %all-to-all-start.5) | async-done | bytes 4194336 | tf_op jit(solution)/shard_map/all_to_all | solution.py:56
  157.5 7.8 reshape.241
  165.3 11.3 %copy.106 = bf16[128,32,2,256]{0,3,1,2:T(8,128)(2,1)} copy(bf16[128,32,2,256]{3,2,1,0:T(2,128)(2,1)} %reshape.241) | data formatting | bytes 8388608 | tf_op jit(solution)/shard_map/reshape | solution.py:37
  183.9 51.2 %all-to-all-done.4 = bf16[16,2,65536]{2,1,0:T(2,128)(2,1)} async-done(((bf16[16,2,65536]{2,1,0:T(2,128)(2,1)}), bf16[16,2,65536]{2,1,0:T(2,128)(2,1)}, u32[]{:S(2)}, u32[]{:S(2)}) %all-to-all-start.4) | async-done | bytes 4194336 | tf_op jit(solution)/shard_map/all_to_all | solution.py:61
  240.9 12.3 %reshape.298 = bf16[64,1,32768]{2,1,0:T(2,128)(2,1)} reshape(bf16[16,2,65536]{2,1,0:T(2,128)(2,1)} %all-to-all-done.4) | data formatting | bytes 8388608
  253.2 26.1 %reduce.4 = bf16[64,32768]{1,0:T(8,128)(2,1)} reduce(bf16[64,1,32768]{2,1,0:T(2,128)(2,1)} %reshape.298, bf16[]{:T(256)} %constant.38), dimensions={1}, to_apply=%all_to_all.87.reduce_sub_computation | reduce | bytes 8388610 | tf_op jit(solution)/shard_map/all_to_all | solution.py:61
  286.5 8.4 reshape.284
  314.2 7.8 reshape.295
  322.0 20.1 %all-to-all-start.6 = ((bf16[16,2,65536]{2,1,0:T(2,128)(2,1)}), bf16[16,2,65536]{2,1,0:T(2,128)(2,1)}, u32[]{:S(2)}, u32[]{:S(2)}) async-start(bf16[16,2,65536]{2,1,0:T(2,128)(2,1)} %reshape.295), calls=%async_computation.6 | async-start | bytes 8388608 | tf_op jit(solution)/shard_map/all_to_all | solution.py:61
  348.9 7.8 reshape.299
  356.8 62.9 %all-to-all-done.6 = bf16[16,2,65536]{2,1,0:T(2,128)(2,1)} async-done(((bf16[16,2,65536]{2,1,0:T(2,128)(2,1)}), bf16[16,2,65536]{2,1,0:T(2,128)(2,1)}, u32[]{:S(2)}, u32[]{:S(2)}) %all-to-all-start.6) | async-done | bytes 4194336 | tf_op jit(solution)/shard_map/all_to_all | solution.py:61
  419.7 19.7 %all-to-all-start.2 = ((bf16[16,2,65536]{2,1,0:T(2,128)(2,1)}), bf16[16,2,65536]{2,1,0:T(2,128)(2,1)}, u32[]{:S(2)}, u32[]{:S(2)}) async-start(bf16[16,2,65536]{2,1,0:T(2,128)(2,1)} %reshape.299), calls=%async_computation.2 | async-start | bytes 8388608 | tf_op jit(solution)/shard_map/all_to_all | solution.py:61
  439.4 12.4 %reshape.296 = bf16[64,1,32768]{2,1,0:T(2,128)(2,1)} reshape(bf16[16,2,65536]{2,1,0:T(2,128)(2,1)} %all-to-all-done.6) | data formatting | bytes 8388608
  451.8 26.1 %reduce.5 = bf16[64,32768]{1,0:T(8,128)(2,1)} reduce(bf16[64,1,32768]{2,1,0:T(2,128)(2,1)} %reshape.296, bf16[]{:T(256)} %constant.38), dimensions={1}, to_apply=%all_to_all.91.reduce_sub_computation | reduce | bytes 8388610 | tf_op jit(solution)/shard_map/all_to_all | solution.py:61
  485.1 8.4 reshape.285
  499.9 17.0 %all-to-all-done.2 = bf16[16,2,65536]{2,1,0:T(2,128)(2,1)} async-done(((bf16[16,2,65536]{2,1,0:T(2,128)(2,1)}), bf16[16,2,65536]{2,1,0:T(2,128)(2,1)}, u32[]{:S(2)}, u32[]{:S(2)}) %all-to-all-start.2) | async-done | bytes 4194336 | tf_op jit(solution)/shard_map/all_to_all | solution.py:61
  516.9 12.4 %reshape.300 = bf16[64,1,32768]{2,1,0:T(2,128)(2,1)} reshape(bf16[16,2,65536]{2,1,0:T(2,128)(2,1)} %all-to-all-done.2) | data formatting | bytes 8388608
  529.3 26.1 %reduce.3 = bf16[64,32768]{1,0:T(8,128)(2,1)} reduce(bf16[64,1,32768]{2,1,0:T(2,128)(2,1)} %reshape.300, bf16[]{:T(256)} %constant.38), dimensions={1}, to_apply=%all_to_all.83.reduce_sub_computation | reduce | bytes 8388610 | tf_op jit(solution)/shard_map/all_to_all | solution.py:61
  562.6 8.4 reshape.283
  588.5 9.4 %scatter_custom_fusion = bf16[1024,2048]{1,0:T(8,128)(2,1)} fusion(s32[768]{0:T(1024)S(1)} %get-tuple-element.29, bf16[768,2048]{1,0:T(8,128)(2,1)S(1)} %reshape.275, bf16[]{:T(256)} %constant.11.clone.1), kind=kCustom, calls=%fused_computation.16 | custom fusion | bytes 4194306 | tf_op jit(solution)/shard_map/scatter | solution.py:112
  601.1 19.6 %all-to-all-start = ((bf16[64,8,2048]{2,1,0:T(8,128)(2,1)}), bf16[64,8,2048]{2,1,0:T(8,128)(2,1)S(1)}, u32[]{:S(2)}, u32[]{:S(2)}) async-start(bf16[64,8,2048]{2,1,0:T(8,128)(2,1)} %constant_dynamic-slice_fusion), calls=%async_computation | async-start | bytes 4194304 | tf_op jit(solution)/shard_map/all_to_all | solution.py:131
  622.4 9.0 %copy.115 = bf16[4,2,256,2048]{3,2,1,0:T(8,128)(2,1)} copy(bf16[4,2,256,2048]{3,2,0,1:T(8,128)(2,1)} %bitcast.131) | data formatting | bytes 16777216 | tf_op jit(solution)/shard_map/reshape | solution.py:125
  631.4 11.4 %copy.120 = bf16[4,512,2048]{2,1,0:T(8,128)(2,1)} copy(bf16[4,512,2048]{1,2,0:T(8,128)(2,1)} %all-gather.10.cloned.1.call-done) | data formatting | bytes 16777216 | tf_op jit(solution)/shard_map/all_gather | solution.py:126
  642.8 18.9 %all-to-all-done = bf16[64,8,2048]{2,1,0:T(8,128)(2,1)S(1)} async-done(((bf16[64,8,2048]{2,1,0:T(8,128)(2,1)}), bf16[64,8,2048]{2,1,0:T(8,128)(2,1)S(1)}, u32[]{:S(2)}, u32[]{:S(2)}) %all-to-all-start) | async-done | bytes 2097184 | tf_op jit(solution)/shard_map/all_to_all | solution.py:131
  661.7 50.0 %all-gather.6.cloned.1.call-done = bf16[4,512,2048]{2,1,0:T(8,128)(2,1)} async-done(((bf16[4,256,2048]{2,1,0:T(8,128)(2,1)}), bf16[4,512,2048]{2,1,0:T(8,128)(2,1)}) %all-gather.6.cloned.1.call-update) | async-done | bytes 8388624 | tf_op jit(solution)/shard_map/all_gather | solution.py:124
  731.5 76.2 %all-gather.12.cloned.1.call-done = bf16[16,1,98304]{2,1,0:T(2,128)(2,1)} async-done(((bf16[1,1,98304]{2,1,0:T(2,128)(2,1)}), bf16[16,1,98304]{2,1,0:T(2,128)(2,1)}) %all-gather.12.cloned.1.call-update) | async-done | bytes 3145744 | tf_op jit(solution)/shard_map/all_gather | solution.py:87
  807.7 18.5 %reduce.7 = bf16[16,98304]{1,0:T(8,128)(2,1)S(1)} reduce(bf16[16,1,98304]{2,1,0:T(2,128)(2,1)} %all-gather.12.cloned.1.call-done, bf16[]{:T(256)} %constant.38), dimensions={1}, to_apply=%all-gather.reduce_sub_computation | reduce | bytes 6291458 | tf_op jit(solution)/shard_map/all_gather | solution.py:87
  (122 shorter events, 225.1 us)
Async XLA Ops:
  44.4 54.5 %all-to-all-start.3 = ((bf16[2,32,32768]{2,1,0:T(8,128)(2,1)}), bf16[2,32,32768]{2,1,0:T(8,128)(2,1)}, u32[]{:S(2)}, u32[]{:S(2)}) async-start(bf16[2,32,32768]{2,1,0:T(8,128)(2,1)} %reshape.247), calls=%async_computation.3 | async-start | bytes 8388608 | tf_op jit(solution)/shard_map/all_to_all | solution.py:49
  98.8 52.7 %all-to-all-start.5 = ((bf16[2,32,32768]{2,1,0:T(8,128)(2,1)}), bf16[2,32,32768]{2,1,0:T(8,128)(2,1)}, u32[]{:S(2)}, u32[]{:S(2)}) async-start(bf16[2,32,32768]{2,1,0:T(8,128)(2,1)} %reshape.254), calls=%async_computation.5 | async-start | bytes 8388608 | tf_op jit(solution)/shard_map/all_to_all | solution.py:56
  151.5 83.5 %all-to-all-start.4 = ((bf16[16,2,65536]{2,1,0:T(2,128)(2,1)}), bf16[16,2,65536]{2,1,0:T(2,128)(2,1)}, u32[]{:S(2)}, u32[]{:S(2)}) async-start(bf16[16,2,65536]{2,1,0:T(2,128)(2,1)} %reshape.297), calls=%async_computation.4 | async-start | bytes 8388608 | tf_op jit(solution)/shard_map/all_to_all | solution.py:61
  235.1 86.9 %all-to-all-start.1 = ((bf16[2,32,32768]{2,1,0:T(8,128)(2,1)}), bf16[2,32,32768]{2,1,0:T(8,128)(2,1)}, u32[]{:S(2)}, u32[]{:S(2)}) async-start(bf16[2,32,32768]{2,1,0:T(8,128)(2,1)} %reshape.242), calls=%async_computation.1 | async-start | bytes 8388608 | tf_op jit(solution)/shard_map/all_to_all | solution.py:42
  240.7 381.7 %all-gather.8.cloned.1.call-start = ((), (), s32[]{:S(2)}) async-start(), calls=%async_computation.11 | async-start | bytes 12582912 | tf_op jit(solution)/shard_map/all_gather | solution.py:125
  322.0 97.6 %all-to-all-start.6 = ((bf16[16,2,65536]{2,1,0:T(2,128)(2,1)}), bf16[16,2,65536]{2,1,0:T(2,128)(2,1)}, u32[]{:S(2)}, u32[]{:S(2)}) async-start(bf16[16,2,65536]{2,1,0:T(2,128)(2,1)} %reshape.295), calls=%async_computation.6 | async-start | bytes 8388608 | tf_op jit(solution)/shard_map/all_to_all | solution.py:61
  419.7 97.2 %all-to-all-start.2 = ((bf16[16,2,65536]{2,1,0:T(2,128)(2,1)}), bf16[16,2,65536]{2,1,0:T(2,128)(2,1)}, u32[]{:S(2)}, u32[]{:S(2)}) async-start(bf16[16,2,65536]{2,1,0:T(2,128)(2,1)} %reshape.299), calls=%async_computation.2 | async-start | bytes 8388608 | tf_op jit(solution)/shard_map/all_to_all | solution.py:61
  439.4 192.0 %all-gather.10.cloned.1.call-start = ((), (), s32[]{:S(2)}) async-start(), calls=%async_computation.12 | async-start | bytes 12582912 | tf_op jit(solution)/shard_map/all_gather | solution.py:126
  499.7 212.0 %all-gather.6.cloned.1.call-start = ((), (), s32[]{:S(2)}) async-start(), calls=%async_computation.10 | async-start | bytes 12582912 | tf_op jit(solution)/shard_map/all_gather | solution.py:124
  575.8 0.7 copy-start.10
  575.8 3.7 copy-start.6
  579.9 0.8 copy-start.5
  597.9 23.2 %copy-start.7 = (f32[128,256]{1,0:T(8,128)S(1)}, f32[128,256]{1,0:T(8,128)}, u32[]{:S(2)}) copy-start(f32[128,256]{1,0:T(8,128)} %param.15) | copy-start | bytes 393220
  597.9 23.2 %copy-start.8 = (f32[128,256]{1,0:T(8,128)S(1)}, f32[128,256]{1,0:T(8,128)}, u32[]{:S(2)}) copy-start(f32[128,256]{1,0:T(8,128)} %param.16) | copy-start | bytes 393220
  597.9 23.2 %copy-start.9 = (f32[128,256]{1,0:T(8,128)S(1)}, f32[128,256]{1,0:T(8,128)}, u32[]{:S(2)}) copy-start(f32[128,256]{1,0:T(8,128)} %param.17) | copy-start | bytes 393220
  597.9 23.3 %copy-start.12 = (f32[128]{0:T(128)S(1)}, f32[128]{0:T(128)}, u32[]{:S(2)}) copy-start(f32[128]{0:T(128)} %param.11) | copy-start | bytes 1540
  601.1 60.6 %all-to-all-start = ((bf16[64,8,2048]{2,1,0:T(8,128)(2,1)}), bf16[64,8,2048]{2,1,0:T(8,128)(2,1)S(1)}, u32[]{:S(2)}, u32[]{:S(2)}) async-start(bf16[64,8,2048]{2,1,0:T(8,128)(2,1)} %constant_dynamic-slice_fusion), calls=%async_computation | async-start | bytes 4194304 | tf_op jit(solution)/shard_map/all_to_all | solution.py:131
  620.7 187.0 %all-gather.12.cloned.1.call-start = ((), (), s32[]{:S(2)}) async-start(), calls=%async_computation.15 | async-start | bytes 6684672 | tf_op jit(solution)/shard_map/all_gather | solution.py:87
  711.7 6.5 copy-start.4
  711.7 9.6 %slice-start = ((s8[8388608]{0:T(1024)(128)(4,1)}), s8[4194304]{0:T(1024)(128)(4,1)S(1)}, s32[]{:S(2)}) async-start(s8[8388608]{0:T(1024)(128)(4,1)} %bitcast.133), calls=%async_computation.16 | async-start | bytes 8388608
  718.1 3.1 slice-start.1
  725.6 110.5 %all-to-all-start.7 = ((bf16[4,128,2048]{2,0,1:T(4,128)(2,1)}), bf16[4,128,2048]{2,0,1:T(4,128)(2,1)}, u32[]{:S(2)}, u32[]{:S(2)}) async-start(bf16[4,128,2048]{2,0,1:T(4,128)(2,1)} %copy.123), calls=%async_computation.7 | async-start | bytes 4194304 | tf_op jit(solution)/shard_map/all_to_all | solution.py:142
  731.3 142.9 %reduce-scatter.5.cloned.1.call-start = ((), (), s32[]{:S(2)}) async-start(), calls=%async_computation.14 | async-start | bytes 1572864 | tf_op jit(solution)/shard_map/reduce_scatter | solution.py:152
  829.1 6.7 copy-start
  829.1 6.9 copy-start.11
  831.0 7.9 copy-start.2
  835.8 44.2 %reduce-scatter.3.cloned.1.call-start = ((), (), s32[]{:S(2)}) async-start(), calls=%async_computation.13 | async-start | bytes 1572864 | tf_op jit(solution)/shard_map/reduce_scatter | solution.py:151
  849.9 9.1 %copy-start.1 = (bf16[1,256,16,128]{1,3,2,0:T(8,128)(2,1)S(1)}, bf16[1,256,16,128]{1,3,2,0:T(8,128)(2,1)}, u32[]{:S(2)}) copy-start(bf16[1,256,16,128]{1,3,2,0:T(8,128)(2,1)} %copy-done) | copy-start | bytes 3145732
  857.5 2.9 copy-start.3
Sparse Core Ops, SparseCore 0:
  307.5 119.3 all-gather.7
  499.8 105.6 all-gather.9
  607.6 103.9 all-gather.5
  714.4 93.3 all-gather.11
  835.9 21.4 reduce-scatter.4
  859.5 20.3 reduce-scatter.2
